TPU v7x, 32 devices: a whole 2x2x4 slice. The times are simulated.
32 devices in a mesh: grp: 2 (over y), ep: 4 (over z), tp: 4 (over x, core).
Axes of the slice: x: 2, y: 2, z: 4, core: 2. Of those that a mesh axis runs over, the one named last changes fastest.
Arguments:
- queries: bfloat16 [1024, 16, 128], P(('grp', 'ep'), 'tp'), parts along dimension 0, may hold values from -6 to 6
- key_vectors: bfloat16 [1024, 16, 128], P(('grp', 'ep'), 'tp'), parts along dimension 0, may hold values from -6 to 6
- values: bfloat16 [1024, 16, 128], P(('grp', 'ep'), 'tp'), parts along dimension 0, may hold values from -6 to 6
- forget_cum: float32 [1024, 16], P('grp', 'tp'), parts along dimension 0, may hold values from -90 to 0, as said below
- query_gain: float32 [128], replicated, may hold values from 0.1 to 5.5
- key_gain: float32 [128], replicated, may hold values from 0.1 to 5.5
- tokens: bfloat16 [4096, 4096], P(('grp', 'ep', 'tp')), parts along dimension 0, may hold values from -6 to 6
- norm_gain: float32 [4096], replicated, may hold values from 0.1 to 1.9
- routes: int32 [4096, 2], P(('grp', 'ep', 'tp')), parts along dimension 0, may hold values from 0 to 127, all different within a row; in each aligned block of 128 rows (0 to 127, 128 to 255, ...) at most 2 rows name the same one
- route_weights: float32 [4096, 2], P(('grp', 'ep', 'tp')), parts along dimension 0, may hold values from 0.3 to 1.2
- expert_gate: bfloat16 [128, 4096, 384], P(('ep', 'tp')), may hold values from -0.09375 to 0.09375
- expert_up: bfloat16 [128, 4096, 384], P(('ep', 'tp')), may hold values from -0.09375 to 0.09375
- expert_down: bfloat16 [128, 384, 4096], P(('ep', 'tp')), may hold values from -0.3125 to 0.3125
- shared_gate: bfloat16 [4096, 192], P(None, 'tp'), may hold values from -0.09375 to 0.09375
- shared_up: bfloat16 [4096, 192], P(None, 'tp'), may hold values from -0.09375 to 0.09375
- shared_down: bfloat16 [192, 4096], P('tp'), may hold values from -0.4375 to 0.4375
Outputs:
- attended: bfloat16 [1024, 16, 128], P(('grp', 'ep'), 'tp'), parts along dimension 0
- routed_output: bfloat16 [4096, 4096], P(('grp', 'ep', 'tp')), parts along dimension 0
There are 2 independent parts, one for each index of `grp`. A program takes and returns all parts, laid end to end along the dimension named above; an argument that names none is the same for every part. Nothing has to cross between parts.
Inputs may be any that keep to these rules, and one draw needn't show every extreme that they name: `routes`: each row names 2 different experts; the rows of one device name every expert exactly 2 times. `forget_cum`: never rises from one position to the next.
All inputs are finite; a program needn't handle non-finite values.
Results may differ from a plain program's by a relative error of at most 0.007.
The roundings to bfloat16 on the way count: a program that leaves them out, or rounds other values in their place, can miss the bound.
Values may be sent and summed in bfloat16 or wider, within the bound.
A program may use at most 128 MiB of HBM per device.

v0:
```python
import functools
import jax
import jax.numpy as jnp
from jax import lax
from jax.experimental import pallas as pl
from jax.experimental.pallas import tpu as pltpu
from jax.sharding import PartitionSpec as P

MESH = pl.DeviceIdType.MESH
F32 = jnp.float32
BF16 = jnp.bfloat16
CAP = 2
GROUPS = 2
HALVES = 2
SENDS = 2
RETURNS = 4
SHARED = 4

D = 4096
EXPERTS = 128
TOP_K = 2


def rms_rows(row_values, gain_vector):
    widened = row_values.astype(jnp.float32)
    inverse = lax.rsqrt(jnp.mean(widened * widened, axis=-1, keepdims=True) + 1e-06)
    return (widened * inverse * gain_vector).astype(jnp.bfloat16)


def attend(queries, key_vectors, values, forget_cum, query_gain, key_gain):
    query_norm = rms_rows(queries, query_gain)
    key_norm = rms_rows(key_vectors, key_gain)
    query_rows = query_norm.shape[0]
    head_count = query_norm.shape[1]
    head_size = query_norm.shape[2]
    first_query = lax.axis_index("ep") * query_rows
    query_positions = first_query + lax.iota(jnp.int32, query_rows)
    last_query = first_query + query_rows - 1
    query_cum = lax.dynamic_slice_in_dim(forget_cum, first_query, query_rows, 0).T
    scale_factor = head_size ** (-0.5)
    start_state = (
        jnp.full((head_count, query_rows), -1e30, jnp.float32),
        jnp.zeros((head_count, query_rows), jnp.float32),
        jnp.zeros((head_count, query_rows, head_size), jnp.float32),
    )
    key_part = lax.all_gather(key_norm, "ep", axis=0, tiled=True)
    value_part = lax.all_gather(values, "ep", axis=0, tiled=True)
    piece_rows = key_part.shape[0]

    def compute(inner_state):
        best_score, denominator, accumulated = inner_state
        cum_block = forget_cum.T
        scores = jnp.einsum(
            "qhd,khd->hqk", query_norm, key_part, preferred_element_type=jnp.float32
        )
        scores = scores * scale_factor + query_cum[:, :, None] - cum_block[:, None, :]
        key_positions = lax.iota(jnp.int32, piece_rows)
        allowed = (key_positions[None, :] <= query_positions[:, None])[None]
        scores = jnp.where(allowed, scores, -1e30)
        new_best = jnp.maximum(best_score, jnp.max(scores, axis=2))
        weights = jnp.where(allowed, jnp.exp(scores - new_best[:, :, None]), 0.0)
        denominator = jnp.sum(weights, axis=2)
        product = jnp.einsum(
            "hqk,khd->hqd",
            weights.astype(jnp.bfloat16),
            value_part,
            preferred_element_type=jnp.float32,
        )
        accumulated = product
        return (new_best, denominator, accumulated)

    best_score, denominator, accumulated = lax.cond(
        jnp.int32(0) <= last_query, compute, lambda inner_state: inner_state, start_state
    )
    return (accumulated / denominator[:, :, None]).transpose(1, 0, 2).astype(jnp.bfloat16)


def shared_expert(normed, shared_gate, shared_up, shared_down):
    row_count = normed.shape[0]
    whole_gate, whole_up, whole_down = (
        lax.all_gather(shared_gate, "tp", axis=1, tiled=True),
        lax.all_gather(shared_up, "tp", axis=1, tiled=True),
        lax.all_gather(shared_down, "tp", axis=0, tiled=True),
    )
    block_total = lax.axis_size("tp")
    gate_values = jnp.dot(normed, whole_gate, preferred_element_type=jnp.float32)
    upward = jnp.dot(normed, whole_up, preferred_element_type=jnp.float32)
    hidden_whole = (jax.nn.silu(gate_values) * upward).astype(jnp.bfloat16)
    part_width = whole_down.shape[0] // block_total
    hidden_blocks = hidden_whole.reshape(row_count, block_total, part_width)
    down_blocks = whole_down.reshape(block_total, part_width, whole_down.shape[1])
    partials = jnp.einsum(
        "rnp,npd->nrd", hidden_blocks, down_blocks, preferred_element_type=jnp.float32
    ).astype(jnp.bfloat16)
    return jnp.sum(partials.astype(jnp.float32), axis=0).astype(jnp.bfloat16)


def mixture(
    tokens,
    norm_gain,
    routes,
    route_weights,
    expert_gate,
    expert_up,
    expert_down,
    shared_gate,
    shared_up,
    shared_down,
):
    normed = rms_rows(tokens, norm_gain)
    row_count = tokens.shape[0]
    shared_out = shared_expert(normed, shared_gate, shared_up, shared_down)
    flat_routes = routes.reshape(-1)
    choice_count = flat_routes.shape[0]
    one_hot = (flat_routes[:, None] == lax.iota(jnp.int32, EXPERTS)[None, :]).astype(jnp.int32)
    slot_rank = jnp.sum((jnp.cumsum(one_hot, axis=0) - one_hot) * one_hot, axis=1)
    slot_index = slot_rank * EXPERTS + flat_routes
    slot_ids = lax.iota(jnp.int32, CAP * EXPERTS)
    matches = slot_index[None, :] == slot_ids[:, None]
    source_row = jnp.sum(
        jnp.where(matches, lax.iota(jnp.int32, choice_count)[None, :] // TOP_K, 0), axis=1
    )
    filled = jnp.any(matches, axis=1)
    outgoing = jnp.where(filled[:, None], normed[source_row], jnp.zeros((), jnp.bfloat16)).reshape(
        CAP, EXPERTS, D
    )
    arrived = lax.all_to_all(outgoing, ("ep", "tp"), split_axis=1, concat_axis=1, tiled=True)
    local_count = expert_gate.shape[0]
    grouped = arrived.reshape(CAP, -1, local_count, D)
    gate_values = jnp.einsum(
        "csed,edf->csef", grouped, expert_gate, preferred_element_type=jnp.float32
    )
    upward = jnp.einsum("csed,edf->csef", grouped, expert_up, preferred_element_type=jnp.float32)
    hidden = (jax.nn.silu(gate_values) * upward).astype(jnp.bfloat16)
    produced = (
        jnp.einsum("csef,efd->csed", hidden, expert_down, preferred_element_type=jnp.float32)
        .astype(jnp.bfloat16)
        .reshape(CAP, -1, D)
    )
    returned = lax.all_to_all(produced, ("ep", "tp"), split_axis=1, concat_axis=1, tiled=True)
    picked_rows = returned.reshape(CAP * EXPERTS, D)[slot_index].reshape(row_count, TOP_K, D)
    routed = jnp.sum(route_weights[:, :, None] * picked_rows.astype(jnp.float32), axis=1)
    return (shared_out.astype(jnp.float32) + routed).astype(jnp.bfloat16)


def local(
    queries,
    key_vectors,
    values,
    forget_cum,
    query_gain,
    key_gain,
    tokens,
    norm_gain,
    routes,
    route_weights,
    expert_gate,
    expert_up,
    expert_down,
    shared_gate,
    shared_up,
    shared_down,
):
    attended = attend(queries, key_vectors, values, forget_cum, query_gain, key_gain)
    routed_output = mixture(
        tokens,
        norm_gain,
        routes,
        route_weights,
        expert_gate,
        expert_up,
        expert_down,
        shared_gate,
        shared_up,
        shared_down,
    )
    return (attended, routed_output)


def rms_heads(wide, gain, heads):
    pieces = []
    for h in range(heads):
        part = wide[:, h, :]
        inverse = lax.rsqrt(jnp.mean(part * part, axis=-1, keepdims=True) + 1e-06)
        pieces.append((part * inverse * gain).astype(BF16))
    return jnp.concatenate(pieces, axis=1)


def iota(shape, axis):
    return lax.broadcasted_iota(jnp.int32, shape, axis)


def fused_kernel(
    n_ep,
    n_tp,
    heads,
    tokens_ref,
    gain_ref,
    routes_ref,
    weights_ref,
    q_ref,
    k_ref,
    v_ref,
    qg_ref,
    kg_ref,
    cum_ref,
    gate_ref,
    up_ref,
    down_ref,
    sg_ref,
    su_ref,
    sd_ref,
    att_ref,
    res_ref,
    tok,
    gain,
    routes,
    weights,
    q_in,
    k_in,
    v_in,
    q_gain,
    k_gain,
    cum,
    normed,
    pick,
    comb,
    gather,
    scatter,
    outgoing,
    x_buf,
    x_rows,
    wide_w,
    down_w,
    y_rows,
    y_buf,
    r_buf,
    sh_buf,
    total,
    qn,
    kv_buf,
    q_far,
    far_out,
    far_in,
    stat_out,
    stat_in,
    in_sem,
    w_sem,
    x_send,
    x_recv,
    x_own,
    y_send,
    y_recv,
    y_own,
    sh_send,
    sh_recv,
    sh_own,
    sf_send,
    sf_recv,
    kv_send,
    kv_recv,
    q_send,
    q_recv,
    far_send,
    far_recv,
    out_sem,
):
    e_pos = lax.axis_index("ep")
    t_pos = lax.axis_index("tp")
    count = n_ep * n_tp
    me = e_pos * n_tp + t_pos
    local_count = gate_ref.shape[0]
    per = local_count // GROUPS
    hidden_width = gate_ref.shape[2]
    block = HALVES * per * CAP
    slots = count * block
    expert_rows = count * CAP
    group_rows = per * expert_rows
    rows, dim = tok.shape
    half = dim // HALVES
    x_wide = half // SENDS
    y_wide = half // RETURNS
    peer_rows = (count - 1) * block

    def device(i):
        return {"ep": i // n_tp, "tp": i % n_tp}

    barrier = pltpu.get_barrier_semaphore()

    def greet(i, carry):
        pl.semaphore_signal(
            barrier, inc=1, device_id=device((me + i) % count), device_id_type=MESH
        )
        return carry

    lax.fori_loop(1, count, greet, 0)
    inputs = [
        pltpu.make_async_copy(src, dst, in_sem.at[i])
        for i, (src, dst) in enumerate(
            (
                (routes_ref, routes),
                (tokens_ref, tok),
                (gain_ref, gain),
                (weights_ref, weights),
                (k_ref, k_in),
                (v_ref, v_in),
                (q_ref, q_in),
                (qg_ref, q_gain),
                (kg_ref, k_gain),
                (cum_ref, cum),
            )
        )
    ]
    for copy in inputs:
        copy.start()

    def weight_copies(g, e):
        n = g * per + e
        return (
            pltpu.make_async_copy(
                gate_ref.at[n], wide_w.at[e, :, pl.ds(0, hidden_width)], w_sem.at[e, 0]
            ),
            pltpu.make_async_copy(
                up_ref.at[n], wide_w.at[e, :, pl.ds(hidden_width, hidden_width)], w_sem.at[e, 1]
            ),
            pltpu.make_async_copy(down_ref.at[n], down_w.at[e], w_sem.at[e, 2]),
        )

    def first_weights(e, carry):
        for copy in weight_copies(0, e):
            copy.start()
        return carry

    shared_refs = (sg_ref, su_ref, sd_ref)
    part = sd_ref.shape[0]
    own_shared = [
        pltpu.make_async_copy(src, sh_buf.at[t_pos, pl.ds(j * part, part)], sh_own.at[j])
        for j, src in enumerate(shared_refs)
    ]

    inputs[0].wait()
    inputs[3].wait()
    lax.fori_loop(0, per, first_weights, 0)
    for copy in own_shared:
        copy.start()

    r = iota((slots, rows), 0)
    which_half = (r % block) // (per * CAP)
    before = jnp.where(iota((rows, rows), 0) < iota((rows, rows), 1), 1.0, 0.0).astype(BF16)

    def chosen(g):
        expert = (r // block) * local_count + g * per + (r % (per * CAP)) // CAP
        first = expert == routes[0:1, :]
        named = jnp.where(first | (expert == routes[1:2, :]), 1.0, 0.0)
        earlier = jnp.dot(named.astype(BF16), before, preferred_element_type=F32)
        return first, jnp.where(earlier == (r % CAP).astype(F32), named, 0.0)

    def fill_pick(g):
        _, hit = chosen(g)
        for h in range(HALVES):
            pick[g, :, h * rows : (h + 1) * rows] = jnp.where(which_half == h, hit, 0.0).astype(
                BF16
            )

    fill_pick(0)
    inputs[1].wait()
    inputs[2].wait()
    wide = tok[...].astype(F32)
    inverse = lax.rsqrt(jnp.mean(wide * wide, axis=-1, keepdims=True) + 1e-06)
    step = half // 4
    for h in range(HALVES):
        for c in range(4):
            cols = slice(h * half + c * step, h * half + (c + 1) * step)
            normed[h * rows : (h + 1) * rows, c * step : (c + 1) * step] = (
                tok[:, cols].astype(F32) * inverse * gain[:, cols]
            ).astype(BF16)
    pl.semaphore_wait(barrier, count - 1)

    def rows_of(i):
        return pl.ds(pl.multiple_of(i * block, block), block)

    across_z = ((e_pos + 2) % n_ep, n_ep - 1 - e_pos, e_pos + 1 - 2 * (e_pos % 2), e_pos)

    def to_peers(src, dst, send_sem, recv_sem):
        for k, e in enumerate(across_z):

            def send(j, carry):
                peer = e * n_tp + (t_pos + j) % n_tp
                pltpu.make_async_remote_copy(
                    src_ref=src.at[rows_of(peer)],
                    dst_ref=dst.at[rows_of(me)],
                    send_sem=send_sem,
                    recv_sem=recv_sem,
                    device_id=device(peer),
                    device_id_type=MESH,
                ).start()
                return carry

            lax.fori_loop(1 if k == 3 else 0, n_tp, send, 0)

    def pick_rows(g, c):
        outgoing[g, c] = jnp.dot(
            pick[g], normed[:, c * x_wide : (c + 1) * x_wide], preferred_element_type=F32
        ).astype(BF16)

    def dispatch(g, c):
        pltpu.make_async_copy(
            outgoing.at[g, c, rows_of(me)], x_buf.at[g, c, rows_of(me)], x_own.at[g, c]
        ).start()
        to_peers(outgoing.at[g, c], x_buf.at[g, c], x_send.at[g], x_recv.at[g])

    mate = t_pos + 1 - 2 * (t_pos % 2)
    across = (t_pos + 2) % n_tp
    sh_wide = dim // SHARED

    def shared_send(c):
        cols = pl.ds(c * sh_wide, sh_wide)
        for s, target in enumerate((mate, across)):
            for j, src in enumerate(shared_refs):
                pltpu.make_async_remote_copy(
                    src_ref=src.at[:, cols],
                    dst_ref=sh_buf.at[t_pos, pl.ds(j * part, part), cols],
                    send_sem=sh_send.at[s, c],
                    recv_sem=sh_recv.at[s, c],
                    device_id={"tp": target},
                    device_id_type=MESH,
                ).start()

    pick_rows(0, 0)
    for c in range(1, SENDS):
        pick_rows(0, c)
        dispatch(0, c - 1)
    for g in range(1, GROUPS):
        fill_pick(g)
    dispatch(0, SENDS - 1)

    for copy in inputs[4:]:
        copy.wait()
    qn[...] = rms_heads(q_in[...].astype(F32), q_gain[...], heads)
    kv_buf[e_pos % 2, 0] = rms_heads(k_in[...].astype(F32), k_gain[...], heads)
    held = v_in[...].astype(F32)
    kv_buf[e_pos % 2, 1] = jnp.concatenate(
        [held[:, h, :].astype(BF16) for h in range(heads)], axis=1
    )

    @pl.when(e_pos % 2 == 0)
    def _():
        kv_buf[1] = jnp.zeros(kv_buf.shape[1:], BF16)

    for g in range(1, GROUPS):
        for c in range(SENDS):
            pick_rows(g, c)

    def kv_copy(j):
        return pltpu.make_async_remote_copy(
            src_ref=kv_buf.at[0, j],
            dst_ref=kv_buf.at[0, j],
            send_sem=kv_send.at[j],
            recv_sem=kv_recv.at[j],
            device_id={"ep": jnp.minimum(e_pos + 1, n_ep - 1)},
            device_id_type=MESH,
        )

    far_index = jnp.maximum(e_pos - 2, 0)

    def q_copy():
        return pltpu.make_async_remote_copy(
            src_ref=qn,
            dst_ref=q_far.at[far_index],
            send_sem=q_send,
            recv_sem=q_recv.at[far_index],
            device_id={"ep": 1},
            device_id_type=MESH,
        )

    @pl.when(e_pos % 2 == 0)
    def _():
        for j in range(2):
            kv_copy(j).start()

    @pl.when(e_pos >= 2)
    def _():
        q_copy().start()

    for g in range(1, GROUPS):
        for c in range(SENDS):
            dispatch(g, c)
    shared_send(0)

    big_row = iota((slots, HALVES * group_rows), 1)
    big_slot = iota((slots, HALVES * group_rows), 0)

    def slot_of(n):
        h = n // group_rows
        e = (n % group_rows) // expert_rows
        src = (n % expert_rows) // CAP
        return src * block + h * (per * CAP) + e * CAP + n % CAP

    scatter[...] = jnp.where(slot_of(big_row) == big_slot, 1.0, 0.0).astype(BF16)
    big_row = iota((HALVES * group_rows, slots), 0)
    big_slot = iota((HALVES * group_rows, slots), 1)
    gather[...] = jnp.where(slot_of(big_row) == big_slot, 1.0, 0.0).astype(BF16)

    for g in range(GROUPS):
        first, hit = chosen(g)
        weight = jnp.where(first, weights[0:1, :], weights[1:2, :]) * hit
        for h in range(HALVES):
            mine = jnp.where(which_half == h, weight, 0.0).T
            high = mine.astype(BF16)
            comb[g, h] = high
            comb[g, HALVES + h] = (mine - high.astype(F32)).astype(BF16)

    size = qn.shape[1] // heads
    contract = (((1,), (1,)), ((), ()))
    diagonal = iota((rows, rows), 0) == iota((rows, rows), 1)

    def column(row):
        return jnp.sum(jnp.where(diagonal, row, 0.0), axis=1, keepdims=True)

    def as_row(col):
        return jnp.sum(jnp.where(diagonal, col, 0.0), axis=0, keepdims=True)

    def span_of(h):
        return slice(h * size, (h + 1) * size)

    def attend_pair(h, q, query_start, key_start, allowed):
        query_span = pl.ds(pl.multiple_of(query_start, rows), rows)
        key_span = pl.ds(pl.multiple_of(key_start, 2 * rows), 2 * rows)
        scores = jnp.concatenate(
            [
                lax.dot_general(
                    q, kv_buf[b, 0, :, span_of(h)], contract, preferred_element_type=F32
                )
                for b in range(2)
            ],
            axis=1,
        )
        scores = (
            scores * (size**-0.5)
            + column(cum[h : h + 1, query_span])
            - cum[h : h + 1, key_span]
        )
        if allowed is not None:
            scores = jnp.where(allowed, scores, -1e30)
        top = jnp.max(scores, axis=1, keepdims=True)
        probs = jnp.exp(scores - top)
        if allowed is not None:
            probs = jnp.where(allowed, probs, 0.0)
        norm = jnp.sum(probs, axis=1, keepdims=True)
        probs = probs.astype(BF16)
        mixed = jnp.dot(
            probs[:, :rows], kv_buf[0, 1, :, span_of(h)], preferred_element_type=F32
        ) + jnp.dot(probs[:, rows:], kv_buf[1, 1, :, span_of(h)], preferred_element_type=F32)
        return top, norm, mixed

    def compute(g):
        pltpu.make_async_copy(
            x_buf.at[g, :, pl.ds(0, peer_rows)],
            x_buf.at[g, :, pl.ds(0, peer_rows)],
            x_recv.at[g],
        ).wait()
        for c in range(SENDS):
            pltpu.make_async_copy(
                x_buf.at[g, c, pl.ds(0, block)], x_buf.at[g, c, pl.ds(0, block)], x_own.at[g, c]
            ).wait()
        for c in range(SENDS):
            ordered = jnp.dot(gather[...], x_buf[g, c], preferred_element_type=F32).astype(BF16)
            for h in range(HALVES):
                start = h * half + c * x_wide
                x_rows[:, start : start + x_wide] = ordered[
                    h * group_rows : (h + 1) * group_rows
                ]

        def one(e, carry):
            copies = weight_copies(g, e)
            span = pl.ds(pl.multiple_of(e * expert_rows, expert_rows), expert_rows)
            copies[0].wait()
            copies[1].wait()
            both = jnp.dot(x_rows[span], wide_w[e], preferred_element_type=F32)
            gate = both[:, :hidden_width]
            hidden = (gate / (1.0 + jnp.exp(-gate)) * both[:, hidden_width:]).astype(BF16)
            copies[2].wait()
            for h in range(HALVES):
                at = pl.ds(pl.multiple_of(h * group_rows + e * expert_rows, expert_rows), expert_rows)
                for c in range(2):
                    cols = slice(c * half // 2, (c + 1) * half // 2)
                    y_rows[at, cols] = jnp.dot(
                        hidden,
                        down_w[e, :, h * half + c * half // 2 : h * half + (c + 1) * half // 2],
                        preferred_element_type=F32,
                    ).astype(BF16)
            if g + 1 < GROUPS:
                for copy in weight_copies(g + 1, e):
                    copy.start()
            return carry

        lax.fori_loop(0, per, one, 0)

    def place(g, c):
        y_buf[g, c] = jnp.dot(
            scatter[...], y_rows[:, c * y_wide : (c + 1) * y_wide], preferred_element_type=F32
        ).astype(BF16)

    def give(g, c):
        pltpu.make_async_copy(
            y_buf.at[g, c, rows_of(me)], r_buf.at[g, c, rows_of(me)], y_own.at[g, c]
        ).start()
        to_peers(y_buf.at[g, c], r_buf.at[g, c], y_send.at[g], y_recv.at[g, c])

    def give_back(g):
        place(g, 0)
        for c in range(1, RETURNS):
            place(g, c)
            give(g, c - 1)

    compute(0)
    give_back(0)
    shared_send(1)

    @pl.when(e_pos % 2 == 1)
    def _():
        for j in range(2):
            kv_copy(j).wait_recv()

    give(0, RETURNS - 1)

    @pl.when(e_pos == 1)
    def _():
        for i in range(2):
            pltpu.make_async_copy(q_far.at[i], q_far.at[i], q_recv.at[i]).wait()
            for h in range(heads):
                top, norm, mixed = attend_pair(
                    h, q_far[i, :, span_of(h)], (2 + i) * rows, 0, None
                )
                far_out[i, :, span_of(h)] = mixed.astype(BF16)
                stat_out[i, h : h + 1] = as_row(top)
                stat_out[i, heads + h : heads + h + 1] = as_row(norm)

    at = (e_pos % 2) * rows + iota((rows, 2 * rows), 0)
    allowed = iota((rows, 2 * rows), 1) <= at
    near = [
        attend_pair(h, qn[:, span_of(h)], e_pos * rows, (e_pos // 2) * 2 * rows, allowed)
        for h in range(heads)
    ]
    for h in range(heads):
        total[:, span_of(h)] = near[h][2]

    def far_copies(i):
        return (
            pltpu.make_async_remote_copy(
                src_ref=far_out.at[i],
                dst_ref=far_in,
                send_sem=far_send.at[i, 0],
                recv_sem=far_recv.at[0],
                device_id={"ep": 2 + i},
                device_id_type=MESH,
            ),
            pltpu.make_async_remote_copy(
                src_ref=stat_out.at[i],
                dst_ref=stat_in,
                send_sem=far_send.at[i, 1],
                recv_sem=far_recv.at[1],
                device_id={"ep": 2 + i},
                device_id_type=MESH,
            ),
        )

    @pl.when(e_pos == 1)
    def _():
        for i in range(2):
            for copy in far_copies(i):
                copy.start()

    shared_send(2)
    compute(1)
    give_back(1)
    shared_send(3)

    @pl.when(e_pos < 2)
    def _():
        far_in[...] = jnp.zeros(far_in.shape, BF16)
        stat_in[0:heads] = jnp.full((heads, rows), -1e30, F32)
        stat_in[heads:] = jnp.zeros((stat_in.shape[0] - heads, rows), F32)

    give(1, RETURNS - 1)

    @pl.when(e_pos >= 2)
    def _():
        for copy in far_copies(0):
            copy.wait_recv()

    parts = []
    for h in range(heads):
        top, norm, _ = near[h]
        far_top = column(stat_in[h : h + 1])
        best = jnp.maximum(top, far_top)
        near_scale = jnp.exp(top - best)
        far_scale = jnp.exp(far_top - best)
        far_norm = column(stat_in[heads + h : heads + h + 1])
        mixed = total[:, span_of(h)] * near_scale + far_in[:, span_of(h)].astype(F32) * far_scale
        parts.append(mixed / (norm * near_scale + far_norm * far_scale))
    att_ref[...] = jnp.stack(parts, axis=1).astype(BF16)

    across_copies = []
    for c in range(SHARED):
        cols = pl.ds(c * sh_wide, sh_wide)
        pltpu.make_async_copy(
            sh_buf.at[across, :, cols], sh_buf.at[across, :, cols], sh_recv.at[1, c]
        ).wait()
        copy = pltpu.make_async_remote_copy(
            src_ref=sh_buf.at[across, :, cols],
            dst_ref=sh_buf.at[across, :, cols],
            send_sem=sf_send.at[c],
            recv_sem=sf_recv.at[c],
            device_id={"tp": mate},
            device_id_type=MESH,
        )
        copy.start()
        across_copies.append(copy)
    for copy in own_shared:
        copy.wait()
    third = mate + 2 - 4 * (mate // 2)
    for c in range(SHARED):
        cols = pl.ds(c * sh_wide, sh_wide)
        pltpu.make_async_copy(
            sh_buf.at[mate, :, cols], sh_buf.at[mate, :, cols], sh_recv.at[0, c]
        ).wait()
        pltpu.make_async_copy(
            sh_buf.at[third, :, cols], sh_buf.at[third, :, cols], sf_recv.at[c]
        ).wait()
    hidden_parts = []
    for blk in range(n_tp):
        both = [
            sum(
                lax.dot_general(
                    normed[h * rows : (h + 1) * rows, :],
                    sh_buf[blk, j * part : (j + 1) * part, h * half : (h + 1) * half],
                    contract,
                    preferred_element_type=F32,
                )
                for h in range(HALVES)
            )
            for j in range(2)
        ]
        hidden_parts.append((both[0] / (1.0 + jnp.exp(-both[0])) * both[1]).astype(BF16))
    narrow = dim // 8
    for c in range(8):
        cols = slice(c * narrow, (c + 1) * narrow)
        summed = jnp.zeros((rows, narrow), F32)
        for blk in range(n_tp):
            piece = jnp.dot(
                hidden_parts[blk],
                sh_buf[blk, 2 * part : 3 * part, cols],
                preferred_element_type=F32,
            )
            summed += piece.astype(BF16).astype(F32)
        total[:, cols] = summed.astype(BF16).astype(F32)

    def returned(g, c):
        pltpu.make_async_copy(
            r_buf.at[g, c, pl.ds(0, peer_rows)],
            r_buf.at[g, c, pl.ds(0, peer_rows)],
            y_recv.at[g, c],
        ).wait()
        pltpu.make_async_copy(
            r_buf.at[g, c, pl.ds(0, block)], r_buf.at[g, c, pl.ds(0, block)], y_own.at[g, c]
        ).wait()
        back = r_buf[g, c]
        for h in range(HALVES):
            cols = slice(h * half + c * y_wide, h * half + (c + 1) * y_wide)
            routed = jnp.dot(comb[g, h], back, preferred_element_type=F32) + jnp.dot(
                comb[g, HALVES + h], back, preferred_element_type=F32
            )
            if g + 1 < GROUPS:
                total[:, cols] += routed
            else:
                tok[:, cols] = (total[:, cols] + routed).astype(BF16)

    for g in range(GROUPS - 1):
        for c in range(RETURNS):
            returned(g, c)
    outs = []
    for c in range(RETURNS):
        returned(GROUPS - 1, c)
        for h in range(HALVES):
            cols = pl.ds(h * half + c * y_wide, y_wide)
            copy = pltpu.make_async_copy(tok.at[:, cols], res_ref.at[:, cols], out_sem.at[c, h])
            copy.start()
            outs.append(copy)

    for g in range(GROUPS):
        pltpu.make_async_copy(
            x_buf.at[g, :, pl.ds(0, peer_rows)],
            x_buf.at[g, :, pl.ds(0, peer_rows)],
            x_send.at[g],
        ).wait()
        pltpu.make_async_copy(
            y_buf.at[g, :, pl.ds(0, peer_rows)],
            y_buf.at[g, :, pl.ds(0, peer_rows)],
            y_send.at[g],
        ).wait()
    for c in range(SHARED):
        cols = pl.ds(c * sh_wide, sh_wide)
        for s in range(2):
            pltpu.make_async_copy(
                sh_buf.at[t_pos, :, cols], sh_buf.at[t_pos, :, cols], sh_send.at[s, c]
            ).wait()
        across_copies[c].wait_send()

    @pl.when(e_pos % 2 == 0)
    def _():
        for j in range(2):
            kv_copy(j).wait_send()

    @pl.when(e_pos >= 2)
    def _():
        q_copy().wait_send()

    @pl.when(e_pos == 1)
    def _():
        for i in range(2):
            for copy in far_copies(i):
                copy.wait_send()

    for copy in outs:
        copy.wait()


def fused_local(n_ep, n_tp, *args):
    (
        queries,
        key_vectors,
        values,
        forget_cum,
        query_gain,
        key_gain,
        tokens,
        norm_gain,
        routes,
        route_weights,
        expert_gate,
        expert_up,
        expert_down,
        shared_gate,
        shared_up,
        shared_down,
    ) = args
    rows, heads, size = queries.shape
    row_count, dim = tokens.shape
    local_count, _, hidden = expert_gate.shape
    count = n_ep * n_tp
    per = local_count // GROUPS
    slots = count * HALVES * per * CAP
    group_rows = count * per * CAP
    half = dim // HALVES
    part = shared_gate.shape[1]
    flat = heads * size
    hbm = pl.BlockSpec(memory_space=pltpu.HBM)
    sds = jax.ShapeDtypeStruct
    vmem = pltpu.VMEM
    dma = pltpu.SemaphoreType.DMA
    attended, routed = pl.pallas_call(
        functools.partial(fused_kernel, n_ep, n_tp, heads),
        out_shape=(sds((rows, heads, size), BF16), sds((row_count, dim), BF16)),
        in_specs=[hbm] * 16,
        out_specs=[pl.BlockSpec(memory_space=pltpu.VMEM), hbm],
        scratch_shapes=[
            vmem((row_count, dim), BF16),
            vmem((1, dim), F32),
            vmem((TOP_K, row_count), jnp.int32),
            vmem((TOP_K, row_count), F32),
            vmem((rows, heads, size), BF16),
            vmem((rows, heads, size), BF16),
            vmem((rows, heads, size), BF16),
            vmem((1, size), F32),
            vmem((1, size), F32),
            vmem((heads, n_ep * rows), F32),
            vmem((HALVES * row_count, half), BF16),
            vmem((GROUPS, slots, HALVES * row_count), BF16),
            vmem((GROUPS, 2 * HALVES, row_count, slots), BF16),
            vmem((HALVES * group_rows, slots), BF16),
            vmem((slots, HALVES * group_rows), BF16),
            vmem((GROUPS, SENDS, slots, half // SENDS), BF16),
            vmem((GROUPS, SENDS, slots, half // SENDS), BF16),
            vmem((group_rows, dim), BF16),
            vmem((per, dim, 2 * hidden), BF16),
            vmem((per, hidden, dim), BF16),
            vmem((HALVES * group_rows, half), BF16),
            vmem((GROUPS, RETURNS, slots, half // RETURNS), BF16),
            vmem((GROUPS, RETURNS, slots, half // RETURNS), BF16),
            vmem((n_tp, 3 * part, dim), BF16),
            vmem((row_count, dim), F32),
            vmem((rows, flat), BF16),
            vmem((2, 2, rows, flat), BF16),
            vmem((2, rows, flat), BF16),
            vmem((2, rows, flat), BF16),
            vmem((rows, flat), BF16),
            vmem((2, 2 * heads, rows), F32),
            vmem((2 * heads, rows), F32),
            dma((10,)),
            dma((per, 3)),
            dma((GROUPS,)),
            dma((GROUPS,)),
            dma((GROUPS, SENDS)),
            dma((GROUPS,)),
            dma((GROUPS, RETURNS)),
            dma((GROUPS, RETURNS)),
            dma((2, SHARED)),
            dma((2, SHARED)),
            dma((3,)),
            dma((SHARED,)),
            dma((SHARED,)),
            dma((2,)),
            dma((2,)),
            dma,
            dma((2,)),
            dma((2, 2)),
            dma((2,)),
            dma((RETURNS, HALVES)),
        ],
        compiler_params=pltpu.CompilerParams(
            collective_id=0, has_side_effects=True, vmem_limit_bytes=60 * 1024 * 1024
        ),
        name="fused",
    )(
        tokens,
        norm_gain.reshape(1, dim),
        routes.T,
        route_weights.T,
        queries,
        key_vectors,
        values,
        query_gain.reshape(1, size),
        key_gain.reshape(1, size),
        forget_cum.T,
        expert_gate,
        expert_up,
        expert_down,
        shared_gate.T,
        shared_up.T,
        shared_down,
    )
    return attended, routed


def local_of(mesh):
    n_ep, n_tp = mesh.shape["ep"], mesh.shape["tp"]

    def run(*args):
        experts = args[10]
        block = CAP * experts.shape[0]
        if n_tp == 4 and n_ep == 4 and block % 16 == 0 and args[15].shape[0] % 16 == 0:
            return fused_local(n_ep, n_tp, *args)
        return local(*args)

    return run


def solution(mesh):
    placed = (
        P(("grp", "ep"), "tp", None),
        P(("grp", "ep"), "tp", None),
        P(("grp", "ep"), "tp", None),
        P("grp", "tp"),
        P(),
        P(),
        P(("grp", "ep", "tp"), None),
        P(),
        P(("grp", "ep", "tp"), None),
        P(("grp", "ep", "tp"), None),
        P(("ep", "tp"), None, None),
        P(("ep", "tp"), None, None),
        P(("ep", "tp"), None, None),
        P(None, "tp"),
        P(None, "tp"),
        P("tp", None),
    )
    return jax.shard_map(
        local_of(mesh),
        mesh=mesh,
        in_specs=placed,
        out_specs=(P(("grp", "ep"), "tp", None), P(("grp", "ep", "tp"), None)),
        check_vma=False,
    )
```

profile of v0, /device:TPU:9, one launch (start us, length us, event | category | flops | bytes accessed | tf_op | source)
XLA Modules:
  0.0 114.7 jit_solution(13642671692377887039)
XLA Ops:
  0.6 110.2 %fused.1 = (bf16[128,4,128]{2,1,0:T(4,128)(2,1)}, bf16[128,4096]{1,0:T(8,128)(2,1)}) custom-call(bf16[128,4096]{1,0:T(8,128)(2,1)} %tokens_ref.1, f32[1,4096]{1,0:T(1,128)} %bitcast.10, s32[2,128]{1,0:T(2,128)} %bitcast.12, f32[2,128]{1,0:T(2,128)} %bitcast.13, bf16[128,4,128]{2,1,0:T(4,128)(2,1)} %q_ref.1, bf16[128,4,128]{2,1,0:T(4,128)(2,1)} %k_ref.1, ...), custom_call_target="tpu_custom_call" | custom-call | tf_op jit(solution)/shard_map/fused/pallas_call | solution.py:862
  110.8 1.6 %copy.20 = bf16[128,4,128]{2,1,0:T(4,128)(2,1)} copy(bf16[128,4,128]{2,1,0:T(4,128)(2,1)} %get-tuple-element.4) | data formatting | bytes 262144
  112.4 2.3 %copy.21 = bf16[128,4096]{1,0:T(8,128)(2,1)} copy(bf16[128,4096]{1,0:T(8,128)(2,1)} %get-tuple-element.5) | data formatting | bytes 2097152
where the time goes:
time: 115 us
  Pallas kernels  110 us (96%)
  local copies, waits for them, and re-layouts  3.89 us (3%)
    pallas_call x1, Pallas kernels, fused_local(): pl.pallas_call(functools.partial(fused_kernel, n_ep, n_tp, heads), out_sh...  110 us
    unnamed x2, local copies, waits for them, and re-layouts  3.89 us

commit v1 on v0

--- a/solution.py
+++ b/solution.py
@@ -12,9 +12,10 @@
 CAP = 2
 GROUPS = 2
 HALVES = 2
-SENDS = 2
+SENDS = 4
 RETURNS = 4
 SHARED = 4
+AHEAD = 3
 
 D = 4096
 EXPERTS = 128
@@ -244,6 +245,7 @@
     far_in,
     stat_out,
     stat_in,
+    near_sum,
     in_sem,
     w_sem,
     x_send,
@@ -263,7 +265,7 @@
     q_recv,
     far_send,
     far_recv,
-    out_sem,
+    credit,
 ):
     e_pos = lax.axis_index("ep")
     t_pos = lax.axis_index("tp")
@@ -407,7 +409,7 @@
         pltpu.make_async_copy(
             outgoing.at[g, c, rows_of(me)], x_buf.at[g, c, rows_of(me)], x_own.at[g, c]
         ).start()
-        to_peers(outgoing.at[g, c], x_buf.at[g, c], x_send.at[g], x_recv.at[g])
+        to_peers(outgoing.at[g, c], x_buf.at[g, c], x_send.at[g, c], x_recv.at[g, c])
 
     mate = t_pos + 1 - 2 * (t_pos % 2)
     across = (t_pos + 2) % n_tp
@@ -426,13 +428,36 @@
                     device_id_type=MESH,
                 ).start()
 
-    pick_rows(0, 0)
-    for c in range(1, SENDS):
-        pick_rows(0, c)
-        dispatch(0, c - 1)
+    order = [(g, c) for g in range(GROUPS) for c in range(SENDS)]
+
+    def arrived(n):
+        g, c = order[n]
+        pltpu.make_async_copy(
+            x_buf.at[g, c, pl.ds(0, peer_rows)],
+            x_buf.at[g, c, pl.ds(0, peer_rows)],
+            x_recv.at[g, c],
+        ).wait()
+        pltpu.make_async_copy(
+            x_buf.at[g, c, pl.ds(0, block)], x_buf.at[g, c, pl.ds(0, block)], x_own.at[g, c]
+        ).wait()
+
+    def sent(g, c):
+        pltpu.make_async_copy(
+            x_buf.at[g, c, pl.ds(0, peer_rows)],
+            x_buf.at[g, c, pl.ds(0, peer_rows)],
+            x_send.at[g, c],
+        ).wait()
+
+    pick_rows(*order[0])
+    for n in range(1, AHEAD):
+        pick_rows(*order[n])
+        dispatch(*order[n - 1])
+    for n in range(AHEAD, SENDS):
+        pick_rows(*order[n])
+    dispatch(*order[AHEAD - 1])
     for g in range(1, GROUPS):
         fill_pick(g)
-    dispatch(0, SENDS - 1)
+    shared_send(0)
 
     for copy in inputs[4:]:
         copy.wait()
@@ -473,20 +498,6 @@
             device_id_type=MESH,
         )
 
-    @pl.when(e_pos % 2 == 0)
-    def _():
-        for j in range(2):
-            kv_copy(j).start()
-
-    @pl.when(e_pos >= 2)
-    def _():
-        q_copy().start()
-
-    for g in range(1, GROUPS):
-        for c in range(SENDS):
-            dispatch(g, c)
-    shared_send(0)
-
     big_row = iota((slots, HALVES * group_rows), 1)
     big_slot = iota((slots, HALVES * group_rows), 0)
 
@@ -509,6 +520,30 @@
             high = mine.astype(BF16)
             comb[g, h] = high
             comb[g, HALVES + h] = (mine - high.astype(F32)).astype(BF16)
+
+    for n in range(SENDS):
+        arrived(n)
+        pl.semaphore_signal(
+            credit,
+            inc=1,
+            device_id={"ep": n_ep - 1 - e_pos, "tp": t_pos},
+            device_id_type=MESH,
+        )
+        pl.semaphore_wait(credit, 1)
+        if n + 1 < SENDS:
+            dispatch(*order[n + AHEAD])
+        else:
+            for m in range(n + AHEAD, len(order)):
+                dispatch(*order[m])
+        if n == 0:
+
+            @pl.when(e_pos % 2 == 0)
+            def _():
+                for j in range(2):
+                    kv_copy(j).start()
+
+        if n == 2:
+            shared_send(1)
 
     size = qn.shape[1] // heads
     contract = (((1,), (1,)), ((), ()))
@@ -554,15 +589,6 @@
         return top, norm, mixed
 
     def compute(g):
-        pltpu.make_async_copy(
-            x_buf.at[g, :, pl.ds(0, peer_rows)],
-            x_buf.at[g, :, pl.ds(0, peer_rows)],
-            x_recv.at[g],
-        ).wait()
-        for c in range(SENDS):
-            pltpu.make_async_copy(
-                x_buf.at[g, c, pl.ds(0, block)], x_buf.at[g, c, pl.ds(0, block)], x_own.at[g, c]
-            ).wait()
         for c in range(SENDS):
             ordered = jnp.dot(gather[...], x_buf[g, c], preferred_element_type=F32).astype(BF16)
             for h in range(HALVES):
@@ -614,15 +640,47 @@
             give(g, c - 1)
 
     compute(0)
-    give_back(0)
-    shared_send(1)
+    shared_send(2)
+    for c in range(RETURNS):
+        place(0, c)
+    sent(GROUPS - 1, SENDS - 2)
+    give(0, 0)
+    sent(GROUPS - 1, SENDS - 1)
+
+    @pl.when(e_pos >= 2)
+    def _():
+        q_copy().start()
+
+    for c in range(1, RETURNS):
+        give(0, c)
 
     @pl.when(e_pos % 2 == 1)
     def _():
         for j in range(2):
             kv_copy(j).wait_recv()
 
-    give(0, RETURNS - 1)
+    at = (e_pos % 2) * rows + iota((rows, 2 * rows), 0)
+    allowed = iota((rows, 2 * rows), 1) <= at
+    near = [
+        attend_pair(h, qn[:, span_of(h)], e_pos * rows, (e_pos // 2) * 2 * rows, allowed)
+        for h in range(heads)
+    ]
+    for h in range(heads):
+        near_sum[:, span_of(h)] = near[h][2]
+
+    shared_send(3)
+    for n in range(SENDS, len(order)):
+        arrived(n)
+    compute(1)
+    give_back(1)
+
+    @pl.when(e_pos < 2)
+    def _():
+        far_in[...] = jnp.zeros(far_in.shape, BF16)
+        stat_in[0:heads] = jnp.full((heads, rows), -1e30, F32)
+        stat_in[heads:] = jnp.zeros((stat_in.shape[0] - heads, rows), F32)
+
+    give(1, RETURNS - 1)
 
     @pl.when(e_pos == 1)
     def _():
@@ -635,15 +693,6 @@
                 far_out[i, :, span_of(h)] = mixed.astype(BF16)
                 stat_out[i, h : h + 1] = as_row(top)
                 stat_out[i, heads + h : heads + h + 1] = as_row(norm)
-
-    at = (e_pos % 2) * rows + iota((rows, 2 * rows), 0)
-    allowed = iota((rows, 2 * rows), 1) <= at
-    near = [
-        attend_pair(h, qn[:, span_of(h)], e_pos * rows, (e_pos // 2) * 2 * rows, allowed)
-        for h in range(heads)
-    ]
-    for h in range(heads):
-        total[:, span_of(h)] = near[h][2]
 
     def far_copies(i):
         return (
@@ -665,42 +714,6 @@
             ),
         )
 
-    @pl.when(e_pos == 1)
-    def _():
-        for i in range(2):
-            for copy in far_copies(i):
-                copy.start()
-
-    shared_send(2)
-    compute(1)
-    give_back(1)
-    shared_send(3)
-
-    @pl.when(e_pos < 2)
-    def _():
-        far_in[...] = jnp.zeros(far_in.shape, BF16)
-        stat_in[0:heads] = jnp.full((heads, rows), -1e30, F32)
-        stat_in[heads:] = jnp.zeros((stat_in.shape[0] - heads, rows), F32)
-
-    give(1, RETURNS - 1)
-
-    @pl.when(e_pos >= 2)
-    def _():
-        for copy in far_copies(0):
-            copy.wait_recv()
-
-    parts = []
-    for h in range(heads):
-        top, norm, _ = near[h]
-        far_top = column(stat_in[h : h + 1])
-        best = jnp.maximum(top, far_top)
-        near_scale = jnp.exp(top - best)
-        far_scale = jnp.exp(far_top - best)
-        far_norm = column(stat_in[heads + h : heads + h + 1])
-        mixed = total[:, span_of(h)] * near_scale + far_in[:, span_of(h)].astype(F32) * far_scale
-        parts.append(mixed / (norm * near_scale + far_norm * far_scale))
-    att_ref[...] = jnp.stack(parts, axis=1).astype(BF16)
-
     across_copies = []
     for c in range(SHARED):
         cols = pl.ds(c * sh_wide, sh_wide)
@@ -717,6 +730,12 @@
         )
         copy.start()
         across_copies.append(copy)
+    @pl.when(e_pos == 1)
+    def _():
+        for i in range(2):
+            for copy in far_copies(i):
+                copy.start()
+
     for copy in own_shared:
         copy.wait()
     third = mate + 2 - 4 * (mate // 2)
@@ -774,26 +793,35 @@
             if g + 1 < GROUPS:
                 total[:, cols] += routed
             else:
-                tok[:, cols] = (total[:, cols] + routed).astype(BF16)
+                res_ref[:, cols] = (total[:, cols] + routed).astype(BF16)
 
     for g in range(GROUPS - 1):
         for c in range(RETURNS):
             returned(g, c)
-    outs = []
+
+    @pl.when(e_pos >= 2)
+    def _():
+        for copy in far_copies(0):
+            copy.wait_recv()
+
+    parts = []
+    for h in range(heads):
+        top, norm, _ = near[h]
+        far_top = column(stat_in[h : h + 1])
+        best = jnp.maximum(top, far_top)
+        near_scale = jnp.exp(top - best)
+        far_scale = jnp.exp(far_top - best)
+        far_norm = column(stat_in[heads + h : heads + h + 1])
+        mixed = near_sum[:, span_of(h)] * near_scale + far_in[:, span_of(h)].astype(F32) * far_scale
+        parts.append(mixed / (norm * near_scale + far_norm * far_scale))
+    att_ref[...] = jnp.stack(parts, axis=1).astype(BF16)
+
     for c in range(RETURNS):
         returned(GROUPS - 1, c)
-        for h in range(HALVES):
-            cols = pl.ds(h * half + c * y_wide, y_wide)
-            copy = pltpu.make_async_copy(tok.at[:, cols], res_ref.at[:, cols], out_sem.at[c, h])
-            copy.start()
-            outs.append(copy)
-
+
+    for g, c in order[: len(order) - 2]:
+        sent(g, c)
     for g in range(GROUPS):
-        pltpu.make_async_copy(
-            x_buf.at[g, :, pl.ds(0, peer_rows)],
-            x_buf.at[g, :, pl.ds(0, peer_rows)],
-            x_send.at[g],
-        ).wait()
         pltpu.make_async_copy(
             y_buf.at[g, :, pl.ds(0, peer_rows)],
             y_buf.at[g, :, pl.ds(0, peer_rows)],
@@ -821,9 +849,6 @@
         for i in range(2):
             for copy in far_copies(i):
                 copy.wait_send()
-
-    for copy in outs:
-        copy.wait()
 
 
 def fused_local(n_ep, n_tp, *args):
@@ -861,9 +886,9 @@
     dma = pltpu.SemaphoreType.DMA
     attended, routed = pl.pallas_call(
         functools.partial(fused_kernel, n_ep, n_tp, heads),
-        out_shape=(sds((rows, heads, size), BF16), sds((row_count, dim), BF16)),
+        out_shape=(vmem((rows, heads, size), BF16), vmem((row_count, dim), BF16)),
         in_specs=[hbm] * 16,
-        out_specs=[pl.BlockSpec(memory_space=pltpu.VMEM), hbm],
+        out_specs=[pl.BlockSpec(memory_space=pltpu.VMEM)] * 2,
         scratch_shapes=[
             vmem((row_count, dim), BF16),
             vmem((1, dim), F32),
@@ -897,10 +922,11 @@
             vmem((rows, flat), BF16),
             vmem((2, 2 * heads, rows), F32),
             vmem((2 * heads, rows), F32),
+            vmem((rows, flat), F32),
             dma((10,)),
             dma((per, 3)),
-            dma((GROUPS,)),
-            dma((GROUPS,)),
+            dma((GROUPS, SENDS)),
+            dma((GROUPS, SENDS)),
             dma((GROUPS, SENDS)),
             dma((GROUPS,)),
             dma((GROUPS, RETURNS)),
@@ -916,7 +942,7 @@
             dma((2,)),
             dma((2, 2)),
             dma((2,)),
-            dma((RETURNS, HALVES)),
+            pltpu.SemaphoreType.REGULAR,
         ],
         compiler_params=pltpu.CompilerParams(
             collective_id=0, has_side_effects=True, vmem_limit_bytes=60 * 1024 * 1024

time: 115 us -> 107 us (0.930); the launches traced: 115 us -> 105 us
  Pallas kernels: 110 us -> 103 us
  local copies, waits for them, and re-layouts: 3.89 us -> 1.63 us
    pallas_call x1, Pallas kernels: 110 us -> 103 us  [fused_local(): pl.pallas_call(functools.partial(fused_kernel, n_ep, n_tp, heads), out_sh...]
    unnamed x2, local copies, waits for them, and re-layouts: 3.89 us -> 1.63 us
where the time goes in v1:
time: 107 us; the launch traced here: 105 us
  Pallas kernels  103 us (96%)
  local copies, waits for them, and re-layouts  1.63 us (2%)
    pallas_call x1, Pallas kernels, fused_local(): pl.pallas_call(functools.partial(fused_kernel, n_ep, n_tp, heads), out_sh...  103 us

profile of v1, /device:TPU:9, one launch (start us, length us, event | category | flops | bytes accessed | tf_op | source)
XLA Modules:
  0.0 105.0 jit_solution(1300666448526438169)
XLA Ops:
  0.6 102.7 %fused.1 = (bf16[128,4,128]{2,1,0:T(4,128)(2,1)S(1)}, bf16[128,4096]{1,0:T(8,128)(2,1)S(1)}) custom-call(bf16[128,4096]{1,0:T(8,128)(2,1)} %tokens_ref.1, f32[1,4096]{1,0:T(1,128)} %bitcast.10, s32[2,128]{1,0:T(2,128)} %bitcast.12, f32[2,128]{1,0:T(2,128)} %bitcast.13, bf16[128,4,128]{2,1,0:T(4,128)(2,1)} %q_ref.1, bf16[128,4,128]{2,1,0:T(4,128)(2,1)} %k_ref.1, ...), custom_call_target="tpu_custom_call" | custom-call | tf_op jit(solution)/shard_map/fused/pallas_call | solution.py:887
  103.3 0.7 copy.20
  104.0 1.0 copy.21

commit v2 on v1

--- a/solution.py
+++ b/solution.py
@@ -250,10 +250,8 @@
     w_sem,
     x_send,
     x_recv,
-    x_own,
     y_send,
     y_recv,
-    y_own,
     sh_send,
     sh_recv,
     sh_own,
@@ -336,7 +334,7 @@
     shared_refs = (sg_ref, su_ref, sd_ref)
     part = sd_ref.shape[0]
     own_shared = [
-        pltpu.make_async_copy(src, sh_buf.at[t_pos, pl.ds(j * part, part)], sh_own.at[j])
+        pltpu.make_async_copy(src, sh_buf.at[t_pos, pl.ds(j * part, part)], sh_own)
         for j, src in enumerate(shared_refs)
     ]
 
@@ -381,10 +379,14 @@
     def rows_of(i):
         return pl.ds(pl.multiple_of(i * block, block), block)
 
-    across_z = ((e_pos + 2) % n_ep, n_ep - 1 - e_pos, e_pos + 1 - 2 * (e_pos % 2), e_pos)
-
-    def to_peers(src, dst, send_sem, recv_sem):
-        for k, e in enumerate(across_z):
+    beside = e_pos + 1 - 2 * (e_pos % 2)
+    opposite = 1 - e_pos // 2
+    inner = opposite + 1
+    outer = opposite * (n_ep - 1)
+    every = ((e_pos + 2) % n_ep, n_ep - 1 - e_pos, beside, e_pos)
+
+    def to_peers(src, dst, send_sem, recv_sem, planes):
+        for e in planes:
 
             def send(j, carry):
                 peer = e * n_tp + (t_pos + j) % n_tp
@@ -398,18 +400,16 @@
                 ).start()
                 return carry
 
-            lax.fori_loop(1 if k == 3 else 0, n_tp, send, 0)
+            lax.fori_loop(1 if e is e_pos else 0, n_tp, send, 0)
 
     def pick_rows(g, c):
         outgoing[g, c] = jnp.dot(
             pick[g], normed[:, c * x_wide : (c + 1) * x_wide], preferred_element_type=F32
         ).astype(BF16)
+        x_buf[g, c, rows_of(me)] = outgoing[g, c, rows_of(me)]
 
     def dispatch(g, c):
-        pltpu.make_async_copy(
-            outgoing.at[g, c, rows_of(me)], x_buf.at[g, c, rows_of(me)], x_own.at[g, c]
-        ).start()
-        to_peers(outgoing.at[g, c], x_buf.at[g, c], x_send.at[g, c], x_recv.at[g, c])
+        to_peers(outgoing.at[g, c], x_buf.at[g, c], x_send.at[g], x_recv.at[g, c], every)
 
     mate = t_pos + 1 - 2 * (t_pos % 2)
     across = (t_pos + 2) % n_tp
@@ -422,8 +422,8 @@
                 pltpu.make_async_remote_copy(
                     src_ref=src.at[:, cols],
                     dst_ref=sh_buf.at[t_pos, pl.ds(j * part, part), cols],
-                    send_sem=sh_send.at[s, c],
-                    recv_sem=sh_recv.at[s, c],
+                    send_sem=sh_send,
+                    recv_sem=sh_recv.at[s],
                     device_id={"tp": target},
                     device_id_type=MESH,
                 ).start()
@@ -432,21 +432,17 @@
 
     def arrived(n):
         g, c = order[n]
-        pltpu.make_async_copy(
-            x_buf.at[g, c, pl.ds(0, peer_rows)],
-            x_buf.at[g, c, pl.ds(0, peer_rows)],
-            x_recv.at[g, c],
-        ).wait()
-        pltpu.make_async_copy(
-            x_buf.at[g, c, pl.ds(0, block)], x_buf.at[g, c, pl.ds(0, block)], x_own.at[g, c]
-        ).wait()
-
-    def sent(g, c):
-        pltpu.make_async_copy(
-            x_buf.at[g, c, pl.ds(0, peer_rows)],
-            x_buf.at[g, c, pl.ds(0, peer_rows)],
-            x_send.at[g, c],
-        ).wait()
+        away = x_buf.at[g, c, pl.ds(0, peer_rows)]
+        pltpu.make_async_copy(away, away, x_recv.at[g, c]).wait()
+
+    def exchange_credit():
+        pl.semaphore_signal(
+            credit,
+            inc=1,
+            device_id={"ep": n_ep - 1 - e_pos, "tp": t_pos},
+            device_id_type=MESH,
+        )
+        pl.semaphore_wait(credit, 1)
 
     pick_rows(*order[0])
     for n in range(1, AHEAD):
@@ -476,12 +472,12 @@
         for c in range(SENDS):
             pick_rows(g, c)
 
-    def kv_copy(j):
+    def kv_copy():
         return pltpu.make_async_remote_copy(
-            src_ref=kv_buf.at[0, j],
-            dst_ref=kv_buf.at[0, j],
-            send_sem=kv_send.at[j],
-            recv_sem=kv_recv.at[j],
+            src_ref=kv_buf.at[0],
+            dst_ref=kv_buf.at[0],
+            send_sem=kv_send,
+            recv_sem=kv_recv,
             device_id={"ep": jnp.minimum(e_pos + 1, n_ep - 1)},
             device_id_type=MESH,
         )
@@ -523,13 +519,7 @@
 
     for n in range(SENDS):
         arrived(n)
-        pl.semaphore_signal(
-            credit,
-            inc=1,
-            device_id={"ep": n_ep - 1 - e_pos, "tp": t_pos},
-            device_id_type=MESH,
-        )
-        pl.semaphore_wait(credit, 1)
+        exchange_credit()
         if n + 1 < SENDS:
             dispatch(*order[n + AHEAD])
         else:
@@ -539,8 +529,11 @@
 
             @pl.when(e_pos % 2 == 0)
             def _():
-                for j in range(2):
-                    kv_copy(j).start()
+                kv_copy().start()
+
+            @pl.when(e_pos >= 2)
+            def _():
+                q_copy().start()
 
         if n == 2:
             shared_send(1)
@@ -626,38 +619,19 @@
         y_buf[g, c] = jnp.dot(
             scatter[...], y_rows[:, c * y_wide : (c + 1) * y_wide], preferred_element_type=F32
         ).astype(BF16)
-
-    def give(g, c):
-        pltpu.make_async_copy(
-            y_buf.at[g, c, rows_of(me)], r_buf.at[g, c, rows_of(me)], y_own.at[g, c]
-        ).start()
-        to_peers(y_buf.at[g, c], r_buf.at[g, c], y_send.at[g], y_recv.at[g, c])
-
-    def give_back(g):
-        place(g, 0)
-        for c in range(1, RETURNS):
-            place(g, c)
-            give(g, c - 1)
+        r_buf[g, c, rows_of(me)] = y_buf[g, c, rows_of(me)]
+
+    def give(g, c, planes):
+        arrival = c if g + 1 == GROUPS else RETURNS
+        to_peers(y_buf.at[g, c], r_buf.at[g, c], y_send.at[g], y_recv.at[arrival], planes)
 
     compute(0)
     shared_send(2)
     for c in range(RETURNS):
         place(0, c)
-    sent(GROUPS - 1, SENDS - 2)
-    give(0, 0)
-    sent(GROUPS - 1, SENDS - 1)
-
-    @pl.when(e_pos >= 2)
-    def _():
-        q_copy().start()
-
-    for c in range(1, RETURNS):
-        give(0, c)
-
     @pl.when(e_pos % 2 == 1)
     def _():
-        for j in range(2):
-            kv_copy(j).wait_recv()
+        kv_copy().wait_recv()
 
     at = (e_pos % 2) * rows + iota((rows, 2 * rows), 0)
     allowed = iota((rows, 2 * rows), 1) <= at
@@ -667,20 +641,6 @@
     ]
     for h in range(heads):
         near_sum[:, span_of(h)] = near[h][2]
-
-    shared_send(3)
-    for n in range(SENDS, len(order)):
-        arrived(n)
-    compute(1)
-    give_back(1)
-
-    @pl.when(e_pos < 2)
-    def _():
-        far_in[...] = jnp.zeros(far_in.shape, BF16)
-        stat_in[0:heads] = jnp.full((heads, rows), -1e30, F32)
-        stat_in[heads:] = jnp.zeros((stat_in.shape[0] - heads, rows), F32)
-
-    give(1, RETURNS - 1)
 
     @pl.when(e_pos == 1)
     def _():
@@ -714,39 +674,57 @@
             ),
         )
 
-    across_copies = []
-    for c in range(SHARED):
-        cols = pl.ds(c * sh_wide, sh_wide)
-        pltpu.make_async_copy(
-            sh_buf.at[across, :, cols], sh_buf.at[across, :, cols], sh_recv.at[1, c]
-        ).wait()
-        copy = pltpu.make_async_remote_copy(
-            src_ref=sh_buf.at[across, :, cols],
-            dst_ref=sh_buf.at[across, :, cols],
-            send_sem=sf_send.at[c],
-            recv_sem=sf_recv.at[c],
-            device_id={"tp": mate},
-            device_id_type=MESH,
-        )
-        copy.start()
-        across_copies.append(copy)
-    @pl.when(e_pos == 1)
+    shared_send(3)
+    for n in range(SENDS, len(order)):
+        arrived(n)
+        if n == SENDS:
+
+            @pl.when(e_pos == 1)
+            def _():
+                for i in range(2):
+                    for copy in far_copies(i):
+                        copy.start()
+
+        if n + 2 == len(order):
+            exchange_credit()
+            give(0, 0, every)
+    exchange_credit()
+    for c in range(1, RETURNS):
+        give(0, c, every)
+    compute(1)
+    first_planes = (outer, beside, e_pos)
+    place(1, 0)
+    for c in range(1, RETURNS):
+        place(1, c)
+        give(1, c - 1, first_planes)
+
+    @pl.when(e_pos < 2)
     def _():
-        for i in range(2):
-            for copy in far_copies(i):
-                copy.start()
-
-    for copy in own_shared:
-        copy.wait()
+        far_in[...] = jnp.zeros(far_in.shape, BF16)
+        stat_in[0:heads] = jnp.full((heads, rows), -1e30, F32)
+        stat_in[heads:] = jnp.zeros((stat_in.shape[0] - heads, rows), F32)
+
+    give(1, RETURNS - 1, first_planes)
+    for c in range(RETURNS):
+        give(1, c, (inner,))
+
+    def whole(i):
+        return sh_buf.at[i]
+
+    pltpu.make_async_copy(whole(across), whole(across), sh_recv.at[1]).wait()
+    across_copy = pltpu.make_async_remote_copy(
+        src_ref=whole(across),
+        dst_ref=whole(across),
+        send_sem=sf_send,
+        recv_sem=sf_recv,
+        device_id={"tp": mate},
+        device_id_type=MESH,
+    )
+    across_copy.start()
+    pltpu.make_async_copy(whole(t_pos), whole(t_pos), sh_own).wait()
     third = mate + 2 - 4 * (mate // 2)
-    for c in range(SHARED):
-        cols = pl.ds(c * sh_wide, sh_wide)
-        pltpu.make_async_copy(
-            sh_buf.at[mate, :, cols], sh_buf.at[mate, :, cols], sh_recv.at[0, c]
-        ).wait()
-        pltpu.make_async_copy(
-            sh_buf.at[third, :, cols], sh_buf.at[third, :, cols], sf_recv.at[c]
-        ).wait()
+    pltpu.make_async_copy(whole(mate), whole(mate), sh_recv.at[0]).wait()
+    pltpu.make_async_copy(whole(third), whole(third), sf_recv).wait()
     hidden_parts = []
     for blk in range(n_tp):
         both = [
@@ -776,14 +754,6 @@
         total[:, cols] = summed.astype(BF16).astype(F32)
 
     def returned(g, c):
-        pltpu.make_async_copy(
-            r_buf.at[g, c, pl.ds(0, peer_rows)],
-            r_buf.at[g, c, pl.ds(0, peer_rows)],
-            y_recv.at[g, c],
-        ).wait()
-        pltpu.make_async_copy(
-            r_buf.at[g, c, pl.ds(0, block)], r_buf.at[g, c, pl.ds(0, block)], y_own.at[g, c]
-        ).wait()
         back = r_buf[g, c]
         for h in range(HALVES):
             cols = slice(h * half + c * y_wide, h * half + (c + 1) * y_wide)
@@ -794,10 +764,6 @@
                 total[:, cols] += routed
             else:
                 res_ref[:, cols] = (total[:, cols] + routed).astype(BF16)
-
-    for g in range(GROUPS - 1):
-        for c in range(RETURNS):
-            returned(g, c)
 
     @pl.when(e_pos >= 2)
     def _():
@@ -816,29 +782,27 @@
         parts.append(mixed / (norm * near_scale + far_norm * far_scale))
     att_ref[...] = jnp.stack(parts, axis=1).astype(BF16)
 
+    away = r_buf.at[0, :, pl.ds(0, peer_rows)]
+    pltpu.make_async_copy(away, away, y_recv.at[RETURNS]).wait()
     for c in range(RETURNS):
-        returned(GROUPS - 1, c)
-
-    for g, c in order[: len(order) - 2]:
-        sent(g, c)
+        returned(0, c)
+
+    for c in range(RETURNS):
+        away = r_buf.at[1, c, pl.ds(0, peer_rows)]
+        pltpu.make_async_copy(away, away, y_recv.at[c]).wait()
+        returned(1, c)
+
     for g in range(GROUPS):
-        pltpu.make_async_copy(
-            y_buf.at[g, :, pl.ds(0, peer_rows)],
-            y_buf.at[g, :, pl.ds(0, peer_rows)],
-            y_send.at[g],
-        ).wait()
-    for c in range(SHARED):
-        cols = pl.ds(c * sh_wide, sh_wide)
-        for s in range(2):
-            pltpu.make_async_copy(
-                sh_buf.at[t_pos, :, cols], sh_buf.at[t_pos, :, cols], sh_send.at[s, c]
-            ).wait()
-        across_copies[c].wait_send()
+        for buf, sem in ((x_buf, x_send), (y_buf, y_send)):
+            away = buf.at[g, :, pl.ds(0, peer_rows)]
+            pltpu.make_async_copy(away, away, sem.at[g]).wait()
+    pair = sh_buf.at[pl.ds(0, 2)]
+    pltpu.make_async_copy(pair, pair, sh_send).wait()
+    across_copy.wait_send()
 
     @pl.when(e_pos % 2 == 0)
     def _():
-        for j in range(2):
-            kv_copy(j).wait_send()
+        kv_copy().wait_send()
 
     @pl.when(e_pos >= 2)
     def _():
@@ -925,19 +889,17 @@
             vmem((rows, flat), F32),
             dma((10,)),
             dma((per, 3)),
-            dma((GROUPS, SENDS)),
-            dma((GROUPS, SENDS)),
+            dma((GROUPS,)),
             dma((GROUPS, SENDS)),
             dma((GROUPS,)),
-            dma((GROUPS, RETURNS)),
-            dma((GROUPS, RETURNS)),
-            dma((2, SHARED)),
-            dma((2, SHARED)),
-            dma((3,)),
-            dma((SHARED,)),
-            dma((SHARED,)),
+            dma((RETURNS + 1,)),
+            dma,
             dma((2,)),
-            dma((2,)),
+            dma,
+            dma,
+            dma,
+            dma,
+            dma,
             dma,
             dma((2,)),
             dma((2, 2)),

time: 107 us -> 105 us (0.981); the launches traced: 105 us -> 105 us
  no operation moved by 1% of the time
where the time goes in v2:
time: 105 us
  Pallas kernels  103 us (98%)
  local copies, waits for them, and re-layouts  1.63 us (2%)
    pallas_call x1, Pallas kernels, fused_local(): pl.pallas_call(functools.partial(fused_kernel, n_ep, n_tp, heads), out_sh...  103 us

profile of v2, /device:TPU:9, one launch (start us, length us, event | category | flops | bytes accessed | tf_op | source)
XLA Modules:
  0.0 105.2 jit_solution(9288426105832650789)
XLA Ops:
  0.6 102.9 %fused.1 = (bf16[128,4,128]{2,1,0:T(4,128)(2,1)S(1)}, bf16[128,4096]{1,0:T(8,128)(2,1)S(1)}) custom-call(bf16[128,4096]{1,0:T(8,128)(2,1)} %tokens_ref.1, f32[1,4096]{1,0:T(1,128)} %bitcast.10, s32[2,128]{1,0:T(2,128)} %bitcast.12, f32[2,128]{1,0:T(2,128)} %bitcast.13, bf16[128,4,128]{2,1,0:T(4,128)(2,1)} %q_ref.1, bf16[128,4,128]{2,1,0:T(4,128)(2,1)} %k_ref.1, ...), custom_call_target="tpu_custom_call" | custom-call | tf_op jit(solution)/shard_map/fused/pallas_call | solution.py:851
  103.6 0.7 copy.20
  104.2 1.0 copy.21

commit v3 on v2

--- a/solution.py
+++ b/solution.py
@@ -383,7 +383,7 @@
     opposite = 1 - e_pos // 2
     inner = opposite + 1
     outer = opposite * (n_ep - 1)
-    every = ((e_pos + 2) % n_ep, n_ep - 1 - e_pos, beside, e_pos)
+    every = (inner, outer, beside, e_pos)
 
     def to_peers(src, dst, send_sem, recv_sem, planes):
         for e in planes:
@@ -674,7 +674,6 @@
             ),
         )
 
-    shared_send(3)
     for n in range(SENDS, len(order)):
         arrived(n)
         if n == SENDS:
@@ -691,6 +690,7 @@
     exchange_credit()
     for c in range(1, RETURNS):
         give(0, c, every)
+    shared_send(3)
     compute(1)
     first_planes = (outer, beside, e_pos)
     place(1, 0)
@@ -813,6 +813,17 @@
         for i in range(2):
             for copy in far_copies(i):
                 copy.wait_send()
+
+
+def finish_kernel(att_ref, res_ref, att_out, res_out, sem):
+    copies = [
+        pltpu.make_async_copy(src, dst, sem.at[i])
+        for i, (src, dst) in enumerate(((res_ref, res_out), (att_ref, att_out)))
+    ]
+    for copy in copies:
+        copy.start()
+    for copy in copies:
+        copy.wait()
 
 
 def fused_local(n_ep, n_tp, *args):
@@ -928,7 +939,17 @@
         shared_up.T,
         shared_down,
     )
-    return attended, routed
+    attended, routed = (
+        pltpu.with_memory_space_constraint(a, pltpu.VMEM) for a in (attended, routed)
+    )
+    return pl.pallas_call(
+        finish_kernel,
+        out_shape=(sds((rows, heads, size), BF16), sds((row_count, dim), BF16)),
+        in_specs=[pl.BlockSpec(memory_space=pltpu.VMEM)] * 2,
+        out_specs=[hbm] * 2,
+        scratch_shapes=[dma((2,))],
+        name="finish",
+    )(attended, routed)
 
 
 def local_of(mesh):

time: 105 us -> 104 us (level)
  local copies, waits for them, and re-layouts: 1.63 us -> 0 us
    unnamed x2 -> x0, local copies, waits for them, and re-layouts: 1.63 us -> none
where the time goes in v3:
time: 104 us
  Pallas kernels  103 us (99%)
    pallas_call x1, Pallas kernels, fused_local(): pl.pallas_call(functools.partial(fused_kernel, n_ep, n_tp, heads), out_sh...  102 us

profile of v3, /device:TPU:9, one launch (start us, length us, event | category | flops | bytes accessed | tf_op | source)
XLA Modules:
  0.0 104.0 jit_solution(14032831142607344978)
XLA Ops:
  0.6 102.2 %fused.1 = (bf16[128,4,128]{2,1,0:T(4,128)(2,1)S(1)}, bf16[128,4096]{1,0:T(8,128)(2,1)S(1)}) custom-call(bf16[128,4096]{1,0:T(8,128)(2,1)} %tokens_ref.1, f32[1,4096]{1,0:T(1,128)} %bitcast.10, s32[2,128]{1,0:T(2,128)} %bitcast.12, f32[2,128]{1,0:T(2,128)} %bitcast.13, bf16[128,4,128]{2,1,0:T(4,128)(2,1)} %q_ref.1, bf16[128,4,128]{2,1,0:T(4,128)(2,1)} %k_ref.1, ...), custom_call_target="tpu_custom_call" | custom-call | tf_op jit(solution)/shard_map/fused/pallas_call | solution.py:862
  102.9 1.0 finish.1

commit v4 on v3

--- a/solution.py
+++ b/solution.py
@@ -264,6 +264,8 @@
     far_send,
     far_recv,
     credit,
+    ready,
+    entered,
 ):
     e_pos = lax.axis_index("ep")
     t_pos = lax.axis_index("tp")
@@ -287,13 +289,26 @@
 
     barrier = pltpu.get_barrier_semaphore()
 
-    def greet(i, carry):
-        pl.semaphore_signal(
-            barrier, inc=1, device_id=device((me + i) % count), device_id_type=MESH
-        )
-        return carry
-
-    lax.fori_loop(1, count, greet, 0)
+    middle = (e_pos == 1) | (e_pos == 2)
+
+    def greet_planes(semaphore, planes):
+        for e in planes:
+
+            def one(j, carry):
+                pl.semaphore_signal(
+                    semaphore,
+                    inc=1,
+                    device_id={"ep": e, "tp": (t_pos + j) % n_tp},
+                    device_id_type=MESH,
+                )
+                return carry
+
+            lax.fori_loop(1 if e is e_pos else 0, n_tp, one, 0)
+
+    @pl.when(middle)
+    def _():
+        greet_planes(barrier, (n_ep - 1 - e_pos, e_pos))
+
     inputs = [
         pltpu.make_async_copy(src, dst, in_sem.at[i])
         for i, (src, dst) in enumerate(
@@ -340,6 +355,17 @@
 
     inputs[0].wait()
     inputs[3].wait()
+
+    @pl.when(middle)
+    def _():
+        pl.semaphore_wait(barrier, 2 * n_tp - 1)
+        greet_planes(barrier, (0, n_ep - 1))
+
+    @pl.when(jnp.logical_not(middle))
+    def _():
+        pl.semaphore_wait(barrier, 2 * n_tp)
+        greet_planes(ready, (1, 2))
+
     lax.fori_loop(0, per, first_weights, 0)
     for copy in own_shared:
         copy.start()
@@ -374,7 +400,6 @@
             normed[h * rows : (h + 1) * rows, c * step : (c + 1) * step] = (
                 tok[:, cols].astype(F32) * inverse * gain[:, cols]
             ).astype(BF16)
-    pl.semaphore_wait(barrier, count - 1)
 
     def rows_of(i):
         return pl.ds(pl.multiple_of(i * block, block), block)
@@ -408,8 +433,8 @@
         ).astype(BF16)
         x_buf[g, c, rows_of(me)] = outgoing[g, c, rows_of(me)]
 
-    def dispatch(g, c):
-        to_peers(outgoing.at[g, c], x_buf.at[g, c], x_send.at[g], x_recv.at[g, c], every)
+    def dispatch(g, c, planes=every):
+        to_peers(outgoing.at[g, c], x_buf.at[g, c], x_send.at[g], x_recv.at[g, c], planes)
 
     mate = t_pos + 1 - 2 * (t_pos % 2)
     across = (t_pos + 2) % n_tp
@@ -445,12 +470,31 @@
         pl.semaphore_wait(credit, 1)
 
     pick_rows(*order[0])
-    for n in range(1, AHEAD):
+    for n in range(1, SENDS):
         pick_rows(*order[n])
-        dispatch(*order[n - 1])
-    for n in range(AHEAD, SENDS):
-        pick_rows(*order[n])
-    dispatch(*order[AHEAD - 1])
+        if n <= AHEAD:
+
+            @pl.when(middle)
+            def _():
+                dispatch(*order[n - 1], (inner, e_pos))
+
+    @pl.when(middle)
+    def _():
+        pl.semaphore_wait(ready, 2 * n_tp)
+        pl.semaphore_signal(
+            entered, inc=1, device_id={"ep": beside, "tp": t_pos}, device_id_type=MESH
+        )
+        for n in range(AHEAD):
+            dispatch(*order[n], (outer, beside))
+
+    @pl.when(jnp.logical_not(middle))
+    def _():
+        for n in range(AHEAD):
+            dispatch(*order[n], (inner, beside))
+        pl.semaphore_wait(entered, 1)
+        for n in range(AHEAD):
+            dispatch(*order[n], (outer, e_pos))
+
     for g in range(1, GROUPS):
         fill_pick(g)
     shared_send(0)
@@ -916,6 +960,8 @@
             dma((2, 2)),
             dma((2,)),
             pltpu.SemaphoreType.REGULAR,
+            pltpu.SemaphoreType.REGULAR,
+            pltpu.SemaphoreType.REGULAR,
         ],
         compiler_params=pltpu.CompilerParams(
             collective_id=0, has_side_effects=True, vmem_limit_bytes=60 * 1024 * 1024

time: 104 us -> 104 us (level)
  no operation moved by 1% of the time
where the time goes in v4:
time: 104 us
  Pallas kernels  103 us (99%)
    pallas_call x1, Pallas kernels, fused_local(): pl.pallas_call(functools.partial(fused_kernel, n_ep, n_tp, heads), out_sh...  102 us

profile of v4, /device:TPU:9, one launch (start us, length us, event | category | flops | bytes accessed | tf_op | source)
XLA Modules:
  0.0 103.6 jit_solution(10795019132827277270)
XLA Ops:
  0.6 101.8 %fused.1 = (bf16[128,4,128]{2,1,0:T(4,128)(2,1)S(1)}, bf16[128,4096]{1,0:T(8,128)(2,1)S(1)}) custom-call(bf16[128,4096]{1,0:T(8,128)(2,1)} %tokens_ref.1, f32[1,4096]{1,0:T(1,128)} %bitcast.10, s32[2,128]{1,0:T(2,128)} %bitcast.12, f32[2,128]{1,0:T(2,128)} %bitcast.13, bf16[128,4,128]{2,1,0:T(4,128)(2,1)} %q_ref.1, bf16[128,4,128]{2,1,0:T(4,128)(2,1)} %k_ref.1, ...), custom_call_target="tpu_custom_call" | custom-call | tf_op jit(solution)/shard_map/fused/pallas_call | solution.py:906
  102.4 1.0 finish.1
